TPU v7x, 32 devices: a whole 2x2x4 slice. The times are simulated.
32 devices in a mesh: sp: 8 (over z, y), tp: 4 (over x, core).
Axes of the slice: x: 2, y: 2, z: 4, core: 2. Of those that a mesh axis runs over, the one named last changes fastest.
Arguments:
- queries: bfloat16 [4096, 2048], P('sp', 'tp'), may hold values from -6 to 6
- keys: bfloat16 [4096, 512], P('sp', 'tp'), may hold values from -6 to 6
- values: bfloat16 [4096, 512], P('sp', 'tp'), may hold values from -6 to 6
- residual: bfloat16 [4096, 2048], P(('sp', 'tp')), may hold values from -0.119628906 to 0.119628906
- out_proj: bfloat16 [2048, 2048], replicated, may hold values from -0.125 to 0.125
- query_gain: float32 [128], replicated, may hold values from 0.7 to 7
- key_gain: float32 [128], replicated, may hold values from 0.7 to 7
- norm_gain: float32 [2048], replicated, may hold values from 0.1 to 1.9
- routes: int32 [4096, 4], P(('sp', 'tp')), may hold values from 0 to 31, all different within a row; in each aligned block of 128 rows (0 to 127, 128 to 255, ...) at most 32 rows name the same one
- route_weight: float32 [4096, 4], P(('sp', 'tp')), may hold values from 0.1 to 1
- expert_gate: bfloat16 [32, 2048, 256], P(('sp', 'tp')), may hold values from -0.125 to 0.125
- expert_up: bfloat16 [32, 2048, 256], P(('sp', 'tp')), may hold values from -0.125 to 0.125
- expert_down: bfloat16 [32, 256, 2048], P(('sp', 'tp')), may hold values from -0.375 to 0.375
- shared_gate: bfloat16 [2048, 256], replicated, may hold values from -0.125 to 0.125
- shared_up: bfloat16 [2048, 256], replicated, may hold values from -0.125 to 0.125
- shared_down: bfloat16 [256, 2048], replicated, may hold values from -0.375 to 0.375
Outputs:
- layer_out: bfloat16 [4096, 2048], P(('sp', 'tp'))
Inputs may be any that keep to these rules, and one draw needn't show every extreme that they name: In the rows of one device (aligned blocks of 128 tokens), no expert is named by more than 32 routes; some expert is named by exactly 32 routes of some device; the 4 experts of a token differ.
All inputs are finite; a program needn't handle non-finite values.
Results may differ from a plain program's by a relative error of at most 0.023.
The roundings to bfloat16 on the way count: a program that leaves them out, or rounds other values in their place, can miss the bound.
Values may be sent and summed in bfloat16 or wider, within the bound.
A program may use at most 128 MiB of HBM per device.

v0:
```python
import math
import jax
import jax.numpy as jnp
from jax import lax
from jax.sharding import PartitionSpec as P

HEADS = 16
KV_HEADS = 4
GRID_W = 64
EPS = 1e-06
THETA = 10000.0


def rotate_pairs(block, cosine, sine):
    first, second = jnp.split(block, 2, axis=-1)
    return jnp.concatenate(
        [first * cosine - second * sine, second * cosine + first * sine], axis=-1
    )


def normed_rotary(source, gain, heads, offset):
    count = source.shape[0]
    width = gain.shape[0]
    values_f = source.astype(jnp.float32).reshape(count, heads, width)
    values_f = (
        values_f * lax.rsqrt(jnp.mean(values_f * values_f, axis=-1, keepdims=True) + EPS) * gain
    )
    position = offset + jnp.arange(count, dtype=jnp.int32)
    grid_row = (position // GRID_W).astype(jnp.float32)
    grid_col = (position % GRID_W).astype(jnp.float32)
    quarter = width // 4
    inverse = jnp.power(THETA, -4.0 * jnp.arange(quarter, dtype=jnp.float32) / width)
    row_angle = (grid_row[:, None] * inverse[None, :])[:, None, :]
    col_angle = (grid_col[:, None] * inverse[None, :])[:, None, :]
    row_half, col_half = jnp.split(values_f, 2, axis=-1)
    turned = jnp.concatenate(
        [
            rotate_pairs(row_half, jnp.cos(row_angle), jnp.sin(row_angle)),
            rotate_pairs(col_half, jnp.cos(col_angle), jnp.sin(col_angle)),
        ],
        axis=-1,
    )
    return turned.reshape(count, heads * width).astype(jnp.bfloat16)


def expert_apply(arrived, expert_gate, expert_up, expert_down):
    sources, slots, width = arrived.shape
    local = expert_gate.shape[0]
    grouped = arrived.reshape(sources // local, local, slots, width)
    gate_part = jnp.einsum(
        "sech,ehf->secf", grouped, expert_gate, preferred_element_type=jnp.float32
    )
    up_part = jnp.einsum("sech,ehf->secf", grouped, expert_up, preferred_element_type=jnp.float32)
    hidden_e = (jax.nn.silu(gate_part) * up_part).astype(jnp.bfloat16)
    result = jnp.einsum("secf,efh->sech", hidden_e, expert_down, preferred_element_type=jnp.float32)
    return result.astype(jnp.bfloat16).reshape(sources, slots, width)


def body(
    queries,
    keys,
    values,
    residual,
    out_proj,
    query_gain,
    key_gain,
    norm_gain,
    routes,
    route_weight,
    expert_gate,
    expert_up,
    expert_down,
    shared_gate,
    shared_up,
    shared_down,
):
    tok_local = queries.shape[0]
    width = query_gain.shape[0]
    group = HEADS // KV_HEADS
    kv_local = keys.shape[1] // width
    scale = 1.0 / math.sqrt(width)
    offset = lax.axis_index("sp") * tok_local
    q_rot = normed_rotary(queries, query_gain, kv_local * group, offset)
    k_rot = normed_rotary(keys, key_gain, kv_local, offset)
    query_3d = q_rot.reshape(tok_local, kv_local, group, width).transpose(1, 2, 0, 3)
    query_3d = query_3d.reshape(kv_local, group * tok_local, width)
    start_state = (
        jnp.full((kv_local, group * tok_local), -jnp.inf, jnp.float32),
        jnp.zeros((kv_local, group * tok_local), jnp.float32),
        jnp.zeros((kv_local, group * tok_local, width), jnp.float32),
    )
    key_piece = lax.all_gather(k_rot, "sp", axis=0, tiled=True)
    value_piece = lax.all_gather(values, "sp", axis=0, tiled=True)
    count = key_piece.shape[0]
    block = math.gcd(count, 512)

    def one_block(index_block, state):
        running_max, running_sum, accum = state
        key_rows = lax.dynamic_slice_in_dim(key_piece, index_block * block, block, 0)
        value_rows = lax.dynamic_slice_in_dim(value_piece, index_block * block, block, 0)
        key_3d = key_rows.reshape(block, kv_local, width)
        value_3d = value_rows.reshape(block, kv_local, width)
        scores = (
            jnp.einsum("gqd,kgd->gqk", query_3d, key_3d, preferred_element_type=jnp.float32) * scale
        )
        new_max = jnp.maximum(running_max, jnp.max(scores, axis=-1))
        weights = jnp.exp(scores - new_max[..., None])
        factor = jnp.exp(running_max - new_max)
        new_sum = running_sum * factor + jnp.sum(weights, axis=-1)
        added = jnp.einsum(
            "gqk,kgd->gqd",
            weights.astype(jnp.bfloat16),
            value_3d,
            preferred_element_type=jnp.float32,
        )
        return (new_max, new_sum, accum * factor[..., None] + added)

    final_max, final_sum, final_acc = lax.fori_loop(0, count // block, one_block, start_state)
    attn_local = (final_acc / final_sum[..., None]).astype(jnp.bfloat16)
    attn_local = attn_local.reshape(kv_local, group, tok_local, width).transpose(2, 0, 1, 3)
    attn_local = attn_local.reshape(tok_local, kv_local * group * width)
    all_heads = lax.all_to_all(attn_local, "tp", split_axis=0, concat_axis=1, tiled=True)
    projected = jnp.dot(all_heads, out_proj, preferred_element_type=jnp.float32)
    hidden1 = (residual.astype(jnp.float32) + projected).astype(jnp.bfloat16)
    hidden_f = hidden1.astype(jnp.float32)
    normed = (
        hidden_f
        * lax.rsqrt(jnp.mean(hidden_f * hidden_f, axis=-1, keepdims=True) + EPS)
        * norm_gain
    ).astype(jnp.bfloat16)
    rows_local = normed.shape[0]
    top_count = routes.shape[1]
    pair_count = rows_local * top_count
    expert_total = expert_gate.shape[0] * lax.axis_size("sp") * lax.axis_size("tp")
    capacity = max(2, 2 * rows_local * top_count // expert_total)
    flat_routes = routes.reshape(pair_count)
    one_hot = (flat_routes[:, None] == jnp.arange(expert_total, dtype=jnp.int32)[None, :]).astype(
        jnp.float32
    )
    lower = (jnp.arange(pair_count)[:, None] >= jnp.arange(pair_count)[None, :]).astype(jnp.float32)
    running_count = jnp.dot(lower, one_hot, precision=lax.Precision.HIGHEST)
    slot_place = (jnp.sum(running_count * one_hot, axis=1) - 1.0).astype(jnp.int32)
    slot_index = flat_routes * capacity + slot_place
    slot_total = expert_total * capacity
    placement = (jnp.arange(slot_total, dtype=jnp.int32)[:, None] == slot_index[None, :]).astype(
        jnp.bfloat16
    )
    placement = jnp.sum(placement.reshape(slot_total, rows_local, top_count), axis=2)
    send_rows = jnp.dot(placement, normed, preferred_element_type=jnp.float32).astype(jnp.bfloat16)
    send_rows = send_rows.reshape(expert_total, capacity, normed.shape[1])
    shared_hidden = (
        jax.nn.silu(jnp.dot(normed, shared_gate, preferred_element_type=jnp.float32))
        * jnp.dot(normed, shared_up, preferred_element_type=jnp.float32)
    ).astype(jnp.bfloat16)
    shared_out = jnp.dot(shared_hidden, shared_down, preferred_element_type=jnp.float32)
    processed = expert_apply(
        lax.all_to_all(send_rows, ("sp", "tp"), split_axis=0, concat_axis=0, tiled=True),
        expert_gate,
        expert_up,
        expert_down,
    )
    returned = lax.all_to_all(processed, ("sp", "tp"), split_axis=0, concat_axis=0, tiled=True)
    returned = returned.reshape(slot_total, normed.shape[1])
    routed = (
        returned[slot_index].reshape(rows_local, top_count, normed.shape[1]).astype(jnp.float32)
    )
    mixed = jnp.einsum("tk,tkd->td", route_weight, routed) + shared_out
    return (hidden_f + mixed).astype(jnp.bfloat16)


def solution(mesh):
    placed = (
        P("sp", "tp"),
        P("sp", "tp"),
        P("sp", "tp"),
        P(("sp", "tp"), None),
        P(),
        P(),
        P(),
        P(),
        P(("sp", "tp"), None),
        P(("sp", "tp"), None),
        P(("sp", "tp"), None, None),
        P(("sp", "tp"), None, None),
        P(("sp", "tp"), None, None),
        P(),
        P(),
        P(),
    )
    return jax.shard_map(
        body, mesh=mesh, in_specs=placed, out_specs=P(("sp", "tp"), None), check_vma=False
    )
```

profile of v0, /device:TPU:0, one launch (start us, length us, event | category | flops | bytes accessed | tf_op | source)
XLA Modules:
  0.0 420.8 jit_solution(3090994777994951920)
XLA Ops:
  19.2 32.9 %all-gather.6.cloned.1.call-done = bf16[4096,1,128]{0,2,1:T(8,128)(2,1)} async-done(((bf16[512,1,128]{0,2,1:T(8,128)(2,1)}), bf16[4096,1,128]{0,2,1:T(8,128)(2,1)}) %all-gather.6.cloned.1.call-update) | async-done | bytes 1048592 | tf_op jit(solution)/shard_map/all_gather | solution.py:92
  52.1 41.4 %all-gather.4.cloned.1.call-done = bf16[4096,128]{1,0:T(8,128)(2,1)} async-done(((bf16[512,128]{1,0:T(8,128)(2,1)}), bf16[4096,128]{1,0:T(8,128)(2,1)}) %all-gather.4.cloned.1.call-update) | async-done | bytes 1048592 | tf_op jit(solution)/shard_map/all_gather | solution.py:93
  93.6 73.7 %while.18 = (s32[]{:T(128)}, f32[1,2048]{1,0:T(1,128)S(1)}, f32[1,2048]{1,0:T(1,128)S(1)}, f32[1,2048,128]{2,1,0:T(8,128)S(1)}, bf16[4096,128]{0,1:T(8,128)(2,1)...) while((s32[]{:T(128)}, f32[1,2048]{1,0:T(1,128)S(1)}, ...), condition=%wide.region_5.6_spmd.clone, body=%wide.region_2.5_spmd.clone.sunk | while | flops 546056192 | bytes 32374984 | solution.py:118
  93.6 3.6 multiply_reduce_fusion.4
  97.2 3.0 fusion.96
  102.8 3.6 multiply_reduce_fusion.4
  106.4 3.0 fusion.96
  112.0 3.6 multiply_reduce_fusion.4
  121.2 3.6 multiply_reduce_fusion.4
  130.4 3.6 multiply_reduce_fusion.4
  139.7 3.6 multiply_reduce_fusion.4
  148.9 3.6 multiply_reduce_fusion.4
  158.1 3.6 multiply_reduce_fusion.4
  169.1 3.7 all-to-all-start
  173.2 8.1 %all-to-all-done = bf16[4,128,512]{2,1,0:T(8,128)(2,1)S(1)} async-done(((bf16[4,128,512]{2,1,0:T(8,128)(2,1)}), bf16[4,128,512]{2,1,0:T(8,128)(2,1)S(1)}, u32[]{:S(2)}, u32[]{:S(2)}) %all-to-all-start) | async-done | bytes 524320 | tf_op jit(solution)/shard_map/all_to_all | solution.py:122
  181.6 4.7 %multiply_reduce_fusion.1 = (f32[128]{0:T(128)S(1)}, f32[128,2048]{1,0:T(8,128)S(1)}) fusion(bf16[128,2048]{0,1:T(8,128)(2,1)S(1)} %bitcast.106, bf16[2048,2048]{1,0:T(8,128)(2,1)} %param.22, bf16[128,2048]{1,0:T(8,128)(2,1)S(1)} %copy-done.5), kind=kOutput, calls=%fused_computation.52 | convolution fusion | flops 1075314560 | bytes 10486272 | tf_op jit(solution)/shard_map/dot_general | solution.py:123
  187.8 95.8 %all_to_all.29 = bf16[32,32,2048]{2,1,0:T(8,128)(2,1)S(1)} all-to-all(bf16[32,32,2048]{2,1,0:T(8,128)(2,1)S(1)} %bitcast.103), channel_id=1, replica_groups=mesh['sp'=8,'tp'=4] {'sp','tp'}, dimensions={0} | all-to-all | bytes 8388608 | tf_op jit(solution)/shard_map/all_to_all | solution.py:157
  287.9 9.1 %convolution_convert_fusion = bf16[32,32,2048]{2,1,0:T(8,128)(2,1)} fusion(bf16[32,32,2048]{2,1,0:T(8,128)(2,1)} %copy-done.2, bf16[1,256,2048]{2,1,0:T(8,128)(2,1)S(1)} %copy-done, bf16[1,2048,256]{2,1,0:T(8,128)(2,1)} %param.29, f32[32,1,32,256]{3,2,0,1:T(8,128)} %convolution_bitcast_fusion.2), kind=kOutput, calls=%fused_computation.23 | convolution fusion | flops 2151153664 | bytes 11534336 | tf_op jit(solution)/shard_map/secf,efh->sech/dot_general | solution.py:55
  297.0 4.0 all-to-all-start.2
  301.7 93.0 %all-to-all-done.2 = bf16[32,32,2048]{2,1,0:T(8,128)(2,1)} async-done(((bf16[32,32,2048]{2,1,0:T(8,128)(2,1)}), bf16[32,32,2048]{2,1,0:T(8,128)(2,1)}, u32[]{:S(2)}, u32[]{:S(2)}) %all-to-all-start.2) | async-done | bytes 4194336 | tf_op jit(solution)/shard_map/all_to_all | solution.py:162
  394.7 8.0 %gather_fusion = bf16[512,2048]{1,0:T(8,128)(2,1)} fusion(bf16[1024,2048]{1,0:T(8,128)(2,1)} %bitcast.29, s32[1024]{0:T(1024)S(1)} %pad_clamp_fusion), kind=kCustom, calls=%fused_computation | custom fusion | bytes 4196352 | tf_op jit(solution)/shard_map/gather | solution.py:165
  402.7 4.2 reshape.478
  406.9 3.8 fusion.76
  410.7 3.3 fusion.19
  (117 shorter events, 59.8 us)
Async XLA Ops:
  6.5 281.3 %copy-start = (bf16[1,256,2048]{2,1,0:T(8,128)(2,1)S(1)}, bf16[1,256,2048]{2,1,0:T(8,128)(2,1)}, u32[]{:S(2)}) copy-start(bf16[1,256,2048]{2,1,0:T(8,128)(2,1)} %param.30) | copy-start | bytes 3145732
  6.5 7.9 %copy-start.9 = (f32[128]{0:T(128)S(1)}, f32[128]{0:T(128)}, u32[]{:S(2)}) copy-start(f32[128]{0:T(128)} %param.23) | copy-start | bytes 1540
  6.5 45.6 %all-gather.6.cloned.1.call-start = ((), (), s32[]{:S(2)}) async-start(), calls=%async_computation.4 | async-start | bytes 1179648 | tf_op jit(solution)/shard_map/all_gather | solution.py:92
  9.7 83.8 %all-gather.4.cloned.1.call-start = ((), (), s32[]{:S(2)}) async-start(), calls=%async_computation.3 | async-start | bytes 1179648 | tf_op jit(solution)/shard_map/all_gather | solution.py:93
  15.2 3.5 copy-start.7
  97.2 3.4 copy-start.1
  106.4 3.4 copy-start.1
  115.6 3.4 copy-start.1
  124.8 3.4 copy-start.1
  134.0 3.4 copy-start.1
  143.3 3.4 copy-start.1
  152.5 3.4 copy-start.1
  161.7 3.4 copy-start.1
  167.3 14.3 %copy-start.5 = (bf16[128,2048]{1,0:T(8,128)(2,1)S(1)}, bf16[128,2048]{1,0:T(8,128)(2,1)}, u32[]{:S(2)}) copy-start(bf16[128,2048]{1,0:T(8,128)(2,1)} %param.21) | copy-start | bytes 1572868
  169.1 12.3 %all-to-all-start = ((bf16[4,128,512]{2,1,0:T(8,128)(2,1)}), bf16[4,128,512]{2,1,0:T(8,128)(2,1)S(1)}, u32[]{:S(2)}, u32[]{:S(2)}) async-start(bf16[4,128,512]{2,1,0:T(8,128)(2,1)} %all_to_all.20), calls=%async_computation | async-start | bytes 1048576 | tf_op jit(solution)/shard_map/all_to_all | solution.py:122
  181.6 4.8 %copy-start.6 = (f32[2048]{0:T(1024)S(1)}, f32[2048]{0:T(1024)}, u32[]{:S(2)}) copy-start(f32[2048]{0:T(1024)} %param.25) | copy-start | bytes 24580
  187.7 97.8 %copy-start.10 = (bf16[1,2048,256]{2,1,0:T(8,128)(2,1)S(1)}, bf16[1,2048,256]{2,1,0:T(8,128)(2,1)}, u32[]{:S(2)}) copy-start(bf16[1,2048,256]{2,1,0:T(8,128)(2,1)} %param.28) | copy-start | bytes 3145732
  283.6 2.0 copy-start.2
  297.0 4.1 copy-start.8
  297.0 4.3 %copy-start.4 = (bf16[2048,256]{1,0:T(8,128)(2,1)S(1)}, bf16[2048,256]{1,0:T(8,128)(2,1)}, u32[]{:S(2)}) copy-start(bf16[2048,256]{1,0:T(8,128)(2,1)} %param.31) | copy-start | bytes 3145732
  297.0 97.7 %all-to-all-start.2 = ((bf16[32,32,2048]{2,1,0:T(8,128)(2,1)}), bf16[32,32,2048]{2,1,0:T(8,128)(2,1)}, u32[]{:S(2)}, u32[]{:S(2)}) async-start(bf16[32,32,2048]{2,1,0:T(8,128)(2,1)} %convolution_convert_fusion), calls=%async_computation.2 | async-start | bytes 8388608 | tf_op jit(solution)/shard_map/all_to_all | solution.py:162
  402.7 8.0 %copy-start.3 = (bf16[256,2048]{1,0:T(8,128)(2,1)S(1)}, bf16[256,2048]{1,0:T(8,128)(2,1)}, u32[]{:S(2)}) copy-start(bf16[256,2048]{1,0:T(8,128)(2,1)} %param.33) | copy-start | bytes 3145732
Sparse Core Ops, SparseCore 0:
  9.9 42.2 all-gather.5
  54.2 39.2 all-gather.3
where the time goes:
time: 422 us; the launch traced here: 421 us
  waiting for transfers between devices  176 us (42%)
  blocking collectives  95.8 us (23%)
  matrix products  71 us (17%)
  other arithmetic  34.1 us (8%)
  local copies, waits for them, and re-layouts  21.8 us (5%)
  between operations  13.7 us (3%)
  starting transfers between devices  7.71 us (2%)
    all_to_all x1, blocking collectives, body(): lax.all_to_all(send_rows, ('sp', 'tp'), split_axis=0, concat_axis=0, tile...  95.8 us
    all_to_all x1, waiting for transfers between devices, body(): lax.all_to_all(processed, ('sp', 'tp'), split_axis=0, concat_axis=0, tile...  93 us
    all_gather x1, waiting for transfers between devices, body(): value_piece = lax.all_gather(values, 'sp', axis=0, tiled=True)  41.4 us
    all_gather x1, waiting for transfers between devices, body(): key_piece = lax.all_gather(k_rot, 'sp', axis=0, tiled=True)  32.9 us
    dot_general x8, matrix products, one_block(): jnp.einsum('gqd,kgd->gqk', query_3d, key_3d, preferred_element_type=jnp.f...  28.8 us
    reduce_sum x8, other arithmetic, one_block(): new_sum = running_sum * factor + jnp.sum(weights, axis=-1)  24.4 us
    dot_general x8, matrix products, one_block(): jnp.einsum('gqk,kgd->gqd', weights.astype(jnp.bfloat16), value_3d, prefer...  17.1 us
    dot_general x1, matrix products, expert_apply(): jnp.einsum('secf,efh->sech', hidden_e, expert_down, preferred_element_typ...  9.08 us
  transfers between devices with their start and end apart: 4, of which 4 were waited for; matrix products, arithmetic and copies ran while one was open for 2% of the time, Pallas kernels for 0%

commit v1 on v0

--- a/solution.py
+++ b/solution.py
@@ -89,8 +89,11 @@
         jnp.zeros((kv_local, group * tok_local), jnp.float32),
         jnp.zeros((kv_local, group * tok_local, width), jnp.float32),
     )
-    key_piece = lax.all_gather(k_rot, "sp", axis=0, tiled=True)
-    value_piece = lax.all_gather(values, "sp", axis=0, tiled=True)
+    key_piece, value_piece = jnp.split(
+        lax.all_gather(jnp.concatenate([k_rot, values], axis=1), "sp", axis=0, tiled=True),
+        [k_rot.shape[1]],
+        axis=1,
+    )
     count = key_piece.shape[0]
     block = math.gcd(count, 512)
 

time: 422 us -> 394 us (0.934)
  waiting for transfers between devices: 176 us -> 146 us
    all_gather x2 -> x1, waiting for transfers between devices: 74.4 us -> 44.5 us  [body(): lax.all_gather(jnp.concatenate([k_rot, values], axis=1), 'sp', axis=0, ti...]
  transfers between devices with their start and end apart: 4 -> 3, of which waited for: 4 -> 3; matrix products, arithmetic and copies ran while one was open for 2% -> 2% of each run, Pallas kernels for 0% -> 0%
where the time goes in v1:
time: 394 us
  waiting for transfers between devices  146 us (37%)
  blocking collectives  95.5 us (24%)
  matrix products  70.7 us (18%)
  other arithmetic  34.2 us (9%)
  local copies, waits for them, and re-layouts  25.9 us (7%)
  between operations  13.7 us (3%)
  starting transfers between devices  7.6 us (2%)
    all_to_all x1, blocking collectives, body(): lax.all_to_all(send_rows, ('sp', 'tp'), split_axis=0, concat_axis=0, tile...  95.5 us
    all_to_all x1, waiting for transfers between devices, body(): lax.all_to_all(processed, ('sp', 'tp'), split_axis=0, concat_axis=0, tile...  93 us
    all_gather x1, waiting for transfers between devices, body(): lax.all_gather(jnp.concatenate([k_rot, values], axis=1), 'sp', axis=0, ti...  44.5 us
    dot_general x8, matrix products, one_block(): jnp.einsum('gqd,kgd->gqk', query_3d, key_3d, preferred_element_type=jnp.f...  28.6 us
    reduce_sum x8, other arithmetic, one_block(): new_sum = running_sum * factor + jnp.sum(weights, axis=-1)  24.4 us
    dot_general x8, matrix products, one_block(): jnp.einsum('gqk,kgd->gqd', weights.astype(jnp.bfloat16), value_3d, prefer...  16.9 us
    dot_general x1, matrix products, expert_apply(): jnp.einsum('secf,efh->sech', hidden_e, expert_down, preferred_element_typ...  9.07 us
    all_to_all x1, waiting for transfers between devices, body(): lax.all_to_all(attn_local, 'tp', split_axis=0, concat_axis=1, tiled=True)  8.13 us
  transfers between devices with their start and end apart: 3, of which 3 were waited for; matrix products, arithmetic and copies ran while one was open for 2% of the time, Pallas kernels for 0%

profile of v1, /device:TPU:0, one launch (start us, length us, event | category | flops | bytes accessed | tf_op | source)
XLA Modules:
  0.0 393.6 jit_solution(12683018205768213622)
XLA Ops:
  19.5 44.5 %all-gather.2.cloned.1.call-done = bf16[4096,256]{0,1:T(8,128)(2,1)} async-done(((bf16[512,256]{0,1:T(8,128)(2,1)}), bf16[4096,256]{0,1:T(8,128)(2,1)}) %all-gather.2.cloned.1.call-update) | async-done | bytes 2097168 | tf_op jit(solution)/shard_map/all_gather | solution.py:93
  64.1 3.1 fusion.76
  67.1 73.4 %while.18 = (s32[]{:T(128)}, f32[1,2048]{1,0:T(1,128)S(1)}, f32[1,2048]{1,0:T(1,128)S(1)}, f32[1,2048,128]{2,1,0:T(8,128)S(1)}, bf16[4096,128]{0,1:T(8,128)(2,1)...) while((s32[]{:T(128)}, f32[1,2048]{1,0:T(1,128)S(1)}, ...), condition=%wide.region_5.6_spmd.clone, body=%wide.region_2.5_spmd.clone.sunk | while | flops 546056192 | bytes 32374992 | solution.py:121
  67.1 3.6 multiply_reduce_fusion.4
  76.3 3.6 multiply_reduce_fusion.4
  85.5 3.6 multiply_reduce_fusion.4
  89.1 3.0 fusion.97
  94.7 3.6 multiply_reduce_fusion.4
  98.3 3.0 fusion.97
  103.8 3.6 multiply_reduce_fusion.4
  113.0 3.6 multiply_reduce_fusion.4
  122.2 3.6 multiply_reduce_fusion.4
  131.4 3.6 multiply_reduce_fusion.4
  142.3 3.7 all-to-all-start
  146.4 8.1 %all-to-all-done = bf16[4,128,512]{2,1,0:T(8,128)(2,1)S(1)} async-done(((bf16[4,128,512]{2,1,0:T(8,128)(2,1)}), bf16[4,128,512]{2,1,0:T(8,128)(2,1)S(1)}, u32[]{:S(2)}, u32[]{:S(2)}) %all-to-all-start) | async-done | bytes 524320 | tf_op jit(solution)/shard_map/all_to_all | solution.py:125
  154.9 4.7 %multiply_reduce_fusion.1 = (f32[128]{0:T(128)S(1)}, f32[128,2048]{1,0:T(8,128)S(1)}) fusion(bf16[128,2048]{0,1:T(8,128)(2,1)S(1)} %bitcast.107, bf16[2048,2048]{1,0:T(8,128)(2,1)} %param.22, bf16[128,2048]{1,0:T(8,128)(2,1)S(1)} %copy-done.5), kind=kOutput, calls=%fused_computation.52 | convolution fusion | flops 1075314560 | bytes 10486272 | tf_op jit(solution)/shard_map/dot_general | solution.py:126
  161.0 95.5 %all_to_all.29 = bf16[32,32,2048]{2,1,0:T(8,128)(2,1)S(1)} all-to-all(bf16[32,32,2048]{2,1,0:T(8,128)(2,1)S(1)} %bitcast.104), channel_id=1, replica_groups=mesh['sp'=8,'tp'=4] {'sp','tp'}, dimensions={0} | all-to-all | bytes 8388608 | tf_op jit(solution)/shard_map/all_to_all | solution.py:160
  260.8 9.1 %convolution_convert_fusion = bf16[32,32,2048]{2,1,0:T(8,128)(2,1)} fusion(bf16[32,32,2048]{2,1,0:T(8,128)(2,1)} %copy-done.2, bf16[1,256,2048]{2,1,0:T(8,128)(2,1)S(1)} %copy-done, bf16[1,2048,256]{2,1,0:T(8,128)(2,1)} %param.29, f32[32,1,32,256]{3,2,0,1:T(8,128)} %convolution_bitcast_fusion.2), kind=kOutput, calls=%fused_computation.23 | convolution fusion | flops 2151153664 | bytes 11534336 | tf_op jit(solution)/shard_map/secf,efh->sech/dot_general | solution.py:55
  269.8 3.9 %all-to-all-start.2 = ((bf16[32,32,2048]{2,1,0:T(8,128)(2,1)}), bf16[32,32,2048]{2,1,0:T(8,128)(2,1)}, u32[]{:S(2)}, u32[]{:S(2)}) async-start(bf16[32,32,2048]{2,1,0:T(8,128)(2,1)} %convolution_convert_fusion), calls=%async_computation.2 | async-start | bytes 8388608 | tf_op jit(solution)/shard_map/all_to_all | solution.py:165
  274.5 93.0 %all-to-all-done.2 = bf16[32,32,2048]{2,1,0:T(8,128)(2,1)} async-done(((bf16[32,32,2048]{2,1,0:T(8,128)(2,1)}), bf16[32,32,2048]{2,1,0:T(8,128)(2,1)}, u32[]{:S(2)}, u32[]{:S(2)}) %all-to-all-start.2) | async-done | bytes 4194336 | tf_op jit(solution)/shard_map/all_to_all | solution.py:165
  367.5 8.0 %gather_fusion = bf16[512,2048]{1,0:T(8,128)(2,1)} fusion(bf16[1024,2048]{1,0:T(8,128)(2,1)} %bitcast.29, s32[1024]{0:T(1024)S(1)} %pad_clamp_fusion), kind=kCustom, calls=%fused_computation | custom fusion | bytes 4196352 | tf_op jit(solution)/shard_map/gather | solution.py:168
  375.5 4.2 %reshape.478 = bf16[128,4,2048]{2,1,0:T(4,128)(2,1)} reshape(bf16[512,2048]{1,0:T(8,128)(2,1)} %gather_fusion) | data formatting | bytes 4194304 | tf_op jit(solution)/shard_map/reshape | solution.py:168
  379.7 3.8 fusion.77
  383.5 3.3 fusion.19
  (117 shorter events, 59.9 us)
Async XLA Ops:
  6.5 254.2 %copy-start = (bf16[1,256,2048]{2,1,0:T(8,128)(2,1)S(1)}, bf16[1,256,2048]{2,1,0:T(8,128)(2,1)}, u32[]{:S(2)}) copy-start(bf16[1,256,2048]{2,1,0:T(8,128)(2,1)} %param.30) | copy-start | bytes 3145732
  6.5 8.3 %copy-start.9 = (f32[128]{0:T(128)S(1)}, f32[128]{0:T(128)}, u32[]{:S(2)}) copy-start(f32[128]{0:T(128)} %param.23) | copy-start | bytes 1540
  6.5 57.5 %all-gather.2.cloned.1.call-start = ((), (), s32[]{:S(2)}) async-start(), calls=%async_computation.3 | async-start | bytes 2359296 | tf_op jit(solution)/shard_map/all_gather | solution.py:93
  15.5 3.5 copy-start.7
  70.7 3.4 copy-start.1
  79.9 3.4 copy-start.1
  89.1 3.4 copy-start.1
  98.2 3.4 copy-start.1
  107.4 3.4 copy-start.1
  116.6 3.4 copy-start.1
  125.8 3.4 copy-start.1
  134.9 3.4 copy-start.1
  140.5 14.3 %copy-start.5 = (bf16[128,2048]{1,0:T(8,128)(2,1)S(1)}, bf16[128,2048]{1,0:T(8,128)(2,1)}, u32[]{:S(2)}) copy-start(bf16[128,2048]{1,0:T(8,128)(2,1)} %param.21) | copy-start | bytes 1572868
  142.3 12.3 %all-to-all-start = ((bf16[4,128,512]{2,1,0:T(8,128)(2,1)}), bf16[4,128,512]{2,1,0:T(8,128)(2,1)S(1)}, u32[]{:S(2)}, u32[]{:S(2)}) async-start(bf16[4,128,512]{2,1,0:T(8,128)(2,1)} %all_to_all.20), calls=%async_computation | async-start | bytes 1048576 | tf_op jit(solution)/shard_map/all_to_all | solution.py:125
  154.8 4.8 %copy-start.6 = (f32[2048]{0:T(1024)S(1)}, f32[2048]{0:T(1024)}, u32[]{:S(2)}) copy-start(f32[2048]{0:T(1024)} %param.25) | copy-start | bytes 24580
  161.0 97.5 %copy-start.10 = (bf16[1,2048,256]{2,1,0:T(8,128)(2,1)S(1)}, bf16[1,2048,256]{2,1,0:T(8,128)(2,1)}, u32[]{:S(2)}) copy-start(bf16[1,2048,256]{2,1,0:T(8,128)(2,1)} %param.28) | copy-start | bytes 3145732
  256.5 2.0 copy-start.2
  269.8 4.1 %copy-start.8 = (f32[128,4]{0,1:T(4,128)S(1)}, f32[128,4]{0,1:T(4,128)}, u32[]{:S(2)}) copy-start(f32[128,4]{0,1:T(4,128)} %param.27) | copy-start | bytes 6148
  269.8 4.3 %copy-start.4 = (bf16[2048,256]{1,0:T(8,128)(2,1)S(1)}, bf16[2048,256]{1,0:T(8,128)(2,1)}, u32[]{:S(2)}) copy-start(bf16[2048,256]{1,0:T(8,128)(2,1)} %param.31) | copy-start | bytes 3145732
  269.8 97.6 %all-to-all-start.2 = ((bf16[32,32,2048]{2,1,0:T(8,128)(2,1)}), bf16[32,32,2048]{2,1,0:T(8,128)(2,1)}, u32[]{:S(2)}, u32[]{:S(2)}) async-start(bf16[32,32,2048]{2,1,0:T(8,128)(2,1)} %convolution_convert_fusion), calls=%async_computation.2 | async-start | bytes 8388608 | tf_op jit(solution)/shard_map/all_to_all | solution.py:165
  375.5 8.0 %copy-start.3 = (bf16[256,2048]{1,0:T(8,128)(2,1)S(1)}, bf16[256,2048]{1,0:T(8,128)(2,1)}, u32[]{:S(2)}) copy-start(bf16[256,2048]{1,0:T(8,128)(2,1)} %param.33) | copy-start | bytes 3145732
Sparse Core Ops, SparseCore 0:
  11.0 53.0 all-gather.1
